TPU v7x, 32 devices: a whole 2x2x4 slice. The times are simulated.
32 devices in a mesh: sp: 8 (over z, x), dp: 4 (over y, core).
Axes of the slice: x: 2, y: 2, z: 4, core: 2. Of those that a mesh axis runs over, the one named last changes fastest.
Arguments:
- tokens: bfloat16 [4, 3072, 2048], P('dp', 'sp'), may hold values from -6 to 6
- q_weight: bfloat16 [2048, 1024], P(('sp', 'dp')), may hold values from -0.13258252 to 0.13258252
- k_weight: bfloat16 [2048, 256], P(('sp', 'dp')), may hold values from -0.13258252 to 0.13258252
- v_weight: bfloat16 [2048, 256], P(('sp', 'dp')), may hold values from -0.125 to 0.125
- out_weight: bfloat16 [1024, 2048], P(None, ('sp', 'dp')), may hold values from -6 to 6
- q_gain: float32 [64], replicated, may hold values from 0.5 to 8
- k_gain: float32 [64], replicated, may hold values from 0.5 to 8
Outputs:
- mixed: bfloat16 [4, 3072, 2048], P('dp', 'sp')
All inputs are finite; a program needn't handle non-finite values.
Results may differ from a plain program's by a relative error of at most 0.0055.
The roundings to bfloat16 on the way count: a program that leaves them out, or rounds other values in their place, can miss the bound.
Values may be sent and summed in bfloat16 or wider, within the bound.
A program may use at most 128 MiB of HBM per device.

v0:
```python
import math
import jax
import jax.numpy as jnp
from jax import lax
from jax.sharding import PartitionSpec as P

GRID_W = 64
epsilon = 1e-06
rope_base = 10000.0


def normalize(tensor, gain_vec):
    mean_sq = jnp.mean(tensor * tensor, axis=-1, keepdims=True)
    return tensor * lax.rsqrt(mean_sq + epsilon) * gain_vec


def rotate(tensor, offset):
    row_count = tensor.shape[0]
    head_width = tensor.shape[2]
    quarter = head_width // 4
    half_width = head_width // 2
    positions = jnp.arange(row_count, dtype=jnp.int32) + offset
    frequency = rope_base ** (-jnp.arange(quarter, dtype=jnp.float32) / quarter)

    def rotate_pair(segment, coords):
        angles = coords.astype(jnp.float32)[:, None] * frequency[None, :]
        cosine = jnp.cos(angles)[:, None, :]
        sine_val = jnp.sin(angles)[:, None, :]
        low_half = segment[..., :quarter]
        high_half = segment[..., quarter:]
        return jnp.concatenate(
            [low_half * cosine - high_half * sine_val, high_half * cosine + low_half * sine_val],
            axis=-1,
        )

    return jnp.concatenate(
        [
            rotate_pair(tensor[..., :half_width], positions // GRID_W),
            rotate_pair(tensor[..., half_width:], positions % GRID_W),
        ],
        axis=-1,
    )


def attend(query_rows, key_rows, value_rows):
    row_count, head_width = query_rows.shape
    block_rows = math.gcd(row_count, 512)
    score_scale = head_width ** (-0.5)

    def attend_block(segment):
        scores = (
            lax.dot_general(
                segment, key_rows, (((1,), (1,)), ((), ())), preferred_element_type=jnp.float32
            )
            * score_scale
        )
        row_max = jnp.max(scores, axis=-1, keepdims=True)
        weights = jnp.exp(scores - row_max)
        shares = (weights / jnp.sum(weights, axis=-1, keepdims=True)).astype(jnp.bfloat16)
        return jnp.dot(shares, value_rows, preferred_element_type=jnp.float32).astype(jnp.bfloat16)

    blocks = query_rows.reshape(row_count // block_rows, block_rows, head_width)
    return lax.map(attend_block, blocks).reshape(row_count, head_width)


def per_device(tokens, q_weight, k_weight, v_weight, out_weight, q_gain, k_gain):
    rows_in = tokens[0]
    tok_count = rows_in.shape[0]
    head_width = q_gain.shape[0]
    q_width = out_weight.shape[0]
    kv_width = k_weight.shape[1]
    q_heads = q_width // head_width
    kv_heads = kv_width // head_width
    group_size = q_heads // kv_heads
    sp_count = lax.axis_size("sp")
    offset = lax.axis_index("sp") * tok_count
    weight_rows = (
        lax.all_gather(q_weight, ("sp", "dp"), axis=0, tiled=True),
        lax.all_gather(k_weight, ("sp", "dp"), axis=0, tiled=True),
        lax.all_gather(v_weight, ("sp", "dp"), axis=0, tiled=True),
    )
    query_raw, key_raw, value_raw = tuple(
        (
            jnp.dot(rows_in, rows_part, preferred_element_type=jnp.float32)
            for rows_part in weight_rows
        )
    )
    queries = rotate(
        normalize(query_raw.reshape(tok_count, q_heads, head_width), q_gain), offset
    ).astype(jnp.bfloat16)
    keys_rot = rotate(
        normalize(key_raw.reshape(tok_count, kv_heads, head_width), k_gain), offset
    ).astype(jnp.bfloat16)
    values_dev = value_raw.astype(jnp.bfloat16)
    keys_wide = jnp.broadcast_to(
        keys_rot[:, :, None, :], (tok_count, kv_heads, group_size, head_width)
    ).reshape(tok_count, q_width)
    values_wide = jnp.broadcast_to(
        values_dev.reshape(tok_count, kv_heads, 1, head_width),
        (tok_count, kv_heads, group_size, head_width),
    ).reshape(tok_count, q_width)
    q_local, k_local, v_local = (
        lax.all_to_all(
            queries.reshape(tok_count, q_width), "sp", split_axis=1, concat_axis=0, tiled=True
        ),
        lax.all_to_all(keys_wide, "sp", split_axis=1, concat_axis=0, tiled=True),
        lax.all_to_all(values_wide, "sp", split_axis=1, concat_axis=0, tiled=True),
    )
    local_heads = q_width // sp_count // head_width
    outputs = []
    for head_index in range(local_heads):
        low_col = head_index * head_width
        outputs.append(
            attend(
                q_local[:, low_col : low_col + head_width],
                k_local[:, low_col : low_col + head_width],
                v_local[:, low_col : low_col + head_width],
            )
        )
    head_results = jnp.concatenate(outputs, axis=1)
    attended = lax.all_to_all(head_results, "sp", split_axis=0, concat_axis=1, tiled=True)
    result = jnp.dot(
        attended,
        lax.all_gather(out_weight, ("sp", "dp"), axis=1, tiled=True),
        preferred_element_type=jnp.float32,
    ).astype(jnp.bfloat16)
    return result[None]


def solution(mesh):
    return jax.shard_map(
        per_device,
        mesh=mesh,
        in_specs=(
            P("dp", "sp", None),
            P(("sp", "dp"), None),
            P(("sp", "dp"), None),
            P(("sp", "dp"), None),
            P(None, ("sp", "dp")),
            P(),
            P(),
        ),
        out_specs=P("dp", "sp", None),
        check_vma=False,
    )
```

profile of v0, /device:TPU:0, one launch (start us, length us, event | category | flops | bytes accessed | tf_op | source)
XLA Modules:
  0.0 334.7 jit_solution(1105141185171821577)
XLA Ops:
  6.5 0.7 all-gather.7.cloned.1.call-update
  9.0 57.6 %all-gather.7.cloned.1.call-done = bf16[2048,256]{1,0:T(8,128)(2,1)} async-done(((bf16[64,256]{1,0:T(8,128)(2,1)}), bf16[2048,256]{1,0:T(8,128)(2,1)}) %all-gather.7.cloned.1.call-update) | async-done | bytes 1048592 | tf_op jit(solution)/shard_map/all_gather | solution.py:79
  66.6 1.5 copy.28
  68.1 0.7 multiply_reduce_fusion.3
  69.1 1.0 broadcast_in_dim.14
  70.1 4.3 %all-to-all-start.1 = ((bf16[384,8,128]{0,2,1:T(8,128)(2,1)}), bf16[384,8,128]{0,2,1:T(8,128)(2,1)S(1)}, u32[]{:S(2)}, u32[]{:S(2)}) async-start(bf16[384,8,128]{0,2,1:T(8,128)(2,1)} %bitcast.14), calls=%async_computation.1 | async-start | bytes 1572864 | tf_op jit(solution)/shard_map/all_to_all | solution.py:106
  74.4 51.6 %all-gather.9.cloned.1.call-done = bf16[2048,256]{1,0:T(8,128)(2,1)} async-done(((bf16[64,256]{1,0:T(8,128)(2,1)}), bf16[2048,256]{1,0:T(8,128)(2,1)}) %all-gather.9.cloned.1.call-update) | async-done | bytes 1048592 | tf_op jit(solution)/shard_map/all_gather | solution.py:80
  126.0 2.0 fusion.27
  128.0 1.0 broadcast_in_dim.16
  129.0 4.3 %all-to-all-start.2 = ((bf16[384,8,128]{0,2,1:T(8,128)(2,1)}), bf16[384,8,128]{0,2,1:T(8,128)(2,1)S(1)}, u32[]{:S(2)}, u32[]{:S(2)}) async-start(bf16[384,8,128]{0,2,1:T(8,128)(2,1)} %bitcast.90), calls=%async_computation.2 | async-start | bytes 1572864 | tf_op jit(solution)/shard_map/all_to_all | solution.py:107
  133.9 1.2 copy.29
  135.1 21.5 %all-to-all-done.2 = bf16[384,8,128]{0,2,1:T(8,128)(2,1)S(1)} async-done(((bf16[384,8,128]{0,2,1:T(8,128)(2,1)}), bf16[384,8,128]{0,2,1:T(8,128)(2,1)S(1)}, u32[]{:S(2)}, u32[]{:S(2)}) %all-to-all-start.2) | async-done | bytes 786464 | tf_op jit(solution)/shard_map/all_to_all | solution.py:107
  156.6 1.2 copy.30
  157.8 35.9 %all-gather.5.cloned.1.call-done = bf16[2048,1024]{1,0:T(8,128)(2,1)} async-done(((bf16[64,1024]{1,0:T(8,128)(2,1)}), bf16[2048,1024]{1,0:T(8,128)(2,1)}) %all-gather.5.cloned.1.call-update) | async-done | bytes 4194320 | tf_op jit(solution)/shard_map/all_gather | solution.py:78
  193.8 6.5 %copy.26 = bf16[1024,2048]{1,0:T(8,128)(2,1)} copy(bf16[1024,2048]{0,1:T(8,128)(2,1)} %bitcast.85) | data formatting | bytes 8388608 | tf_op jit(solution)/shard_map/dot_general | solution.py:84
  200.3 4.6 %multiply_reduce_fusion.2 = (f32[384,16]{0,1:T(8,128)S(1)}, f32[384,16,64]{0,2,1:T(8,128)S(1)}) fusion(bf16[16,64,2048]{2,1,0:T(8,128)(2,1)} %bitcast.86, bf16[1,384,2048]{2,1,0:T(8,128)(2,1)S(1)} %copy-done), kind=kOutput, calls=%fused_computation.35 | convolution fusion | flops 1611393024 | bytes 7364608 | tf_op jit(solution)/shard_map/dot_general | solution.py:84
  205.6 1.2 copy.27
  206.7 4.4 %all-to-all-start = ((bf16[384,8,128]{2,0,1:T(8,128)(2,1)}), bf16[384,8,128]{2,0,1:T(8,128)(2,1)}, u32[]{:S(2)}, u32[]{:S(2)}) async-start(bf16[384,8,128]{2,0,1:T(8,128)(2,1)} %copy.27), calls=%async_computation | async-start | bytes 1572864 | tf_op jit(solution)/shard_map/all_to_all | solution.py:103
  211.2 1.7 fusion.36
  212.9 2.8 fusion.35
  215.7 20.6 %all-to-all-done = bf16[384,8,128]{2,0,1:T(8,128)(2,1)} async-done(((bf16[384,8,128]{2,0,1:T(8,128)(2,1)}), bf16[384,8,128]{2,0,1:T(8,128)(2,1)}, u32[]{:S(2)}, u32[]{:S(2)}) %all-to-all-start) | async-done | bytes 786464 | tf_op jit(solution)/shard_map/all_to_all | solution.py:103
  236.3 2.9 fusion.37
  239.2 28.8 %while.20 = (s32[]{:T(128)}, bf16[6,512,64]{1,2,0:T(8,128)(2,1)S(1)}, bf16[6,512,64]{2,1,0:T(8,128)(2,1)}, bf16[3072,64]{1,0:T(8,128)(2,1)S(1)}, bf16[3072,64]{1,0:T(8,128)(2,1)}, /*index=5*/s32[]{:T(128)}) while((s32[]{:T(128)}, bf16[6,512,64]{1,2,0:T(8,128)(2,1)S(1)}, bf16[6,512,64]{2,1,0:T(8,128)(2,1)}, bf16[3072,64]{1,0:T(8,128)(2,1)S(1)}, ...), condition=%wide.region_5.6_spmd, body=%wide.region_2.5_spmd.sunk | while | flops 416840704 | bytes 21834340 | solution.py:63
  239.3 2.0 multiply_reduce_fusion.6
  241.2 1.2 fusion.57
  242.4 1.6 fusion.58
  244.0 2.0 multiply_reduce_fusion.6
  246.1 1.2 fusion.57
  247.2 1.6 fusion.58
  248.9 2.0 multiply_reduce_fusion.6
  250.9 1.2 fusion.57
  252.0 1.6 fusion.58
  253.7 2.0 multiply_reduce_fusion.6
  255.7 1.2 fusion.57
  256.8 1.6 fusion.58
  258.5 2.0 multiply_reduce_fusion.6
  260.5 1.2 fusion.57
  261.7 1.6 fusion.58
  263.3 2.0 multiply_reduce_fusion.6
  265.3 1.2 fusion.57
  266.4 1.6 fusion.58
  268.6 28.7 %while.21 = (s32[]{:T(128)}, bf16[6,512,64]{1,2,0:T(8,128)(2,1)S(1)}, bf16[6,512,64]{2,1,0:T(8,128)(2,1)}, bf16[3072,64]{1,0:T(8,128)(2,1)S(1)}, bf16[3072,64]{1,0:T(8,128)(2,1)}, /*index=5*/s32[]{:T(128)}) while((s32[]{:T(128)}, bf16[6,512,64]{1,2,0:T(8,128)(2,1)S(1)}, bf16[6,512,64]{2,1,0:T(8,128)(2,1)}, bf16[3072,64]{1,0:T(8,128)(2,1)S(1)}, ...), condition=%wide.region_9.10_spmd, body=%wide.region_6.9_spmd.sunk | while | flops 416840704 | bytes 21834340 | solution.py:63
  268.6 2.0 multiply_reduce_fusion.7
  270.6 1.2 fusion.61
  271.8 1.6 fusion.62
  273.4 2.0 multiply_reduce_fusion.7
  275.4 1.2 fusion.61
  276.5 1.6 fusion.62
  278.2 2.0 multiply_reduce_fusion.7
  280.2 1.2 fusion.61
  281.3 1.6 fusion.62
  283.0 2.0 multiply_reduce_fusion.7
  285.0 1.2 fusion.61
  286.1 1.6 fusion.62
  287.8 2.0 multiply_reduce_fusion.7
  289.8 1.2 fusion.61
  290.9 1.6 fusion.62
  292.6 2.0 multiply_reduce_fusion.7
  294.5 1.2 fusion.61
  295.7 1.6 fusion.62
  297.9 1.0 copy.33
  298.9 3.7 %all-to-all-start.3 = ((bf16[8,384,128]{1,2,0:T(8,128)(2,1)}), bf16[8,384,128]{1,2,0:T(8,128)(2,1)S(1)}, u32[]{:S(2)}, u32[]{:S(2)}) async-start(bf16[8,384,128]{1,2,0:T(8,128)(2,1)} %copy.33), calls=%async_computation.3 | async-start | bytes 1572864 | tf_op jit(solution)/shard_map/all_to_all | solution.py:121
  302.6 20.4 %all-to-all-done.3 = bf16[8,384,128]{1,2,0:T(8,128)(2,1)S(1)} async-done(((bf16[8,384,128]{1,2,0:T(8,128)(2,1)}), bf16[8,384,128]{1,2,0:T(8,128)(2,1)S(1)}, u32[]{:S(2)}, u32[]{:S(2)}) %all-to-all-start.3) | async-done | bytes 786464 | tf_op jit(solution)/shard_map/all_to_all | solution.py:121
  323.0 5.2 %fusion.20 = bf16[1,384,2048]{2,1,0:T(8,128)(2,1)} fusion(bf16[384,1024]{0,1:T(8,128)(2,1)S(1)} %bitcast.95, bf16[1024,2048]{0,1:T(8,128)(2,1)} %all-gather.11.cloned.1.call-done), kind=kOutput, calls=%fused_computation.27 | convolution fusion | flops 1611399168 | bytes 6553600 | tf_op jit(solution)/shard_map/dot_general | solution.py:122
  (57 shorter events, 4.4 us)
Async XLA Ops:
  6.5 61.6 %copy-start = (bf16[1,384,2048]{2,1,0:T(8,128)(2,1)S(1)}, bf16[1,384,2048]{2,1,0:T(8,128)(2,1)}, u32[]{:S(2)}) copy-start(bf16[1,384,2048]{2,1,0:T(8,128)(2,1)} %param.11) | copy-start | bytes 4718596
  6.5 62.4 %copy-start.3 = (f32[64]{0:T(128)S(1)}, f32[64]{0:T(128)}, u32[]{:S(2)}) copy-start(f32[64]{0:T(128)} %param.17) | copy-start | bytes 772
  6.5 60.1 %all-gather.7.cloned.1.call-start = ((), (), s32[]{:S(2)}) async-start(), calls=%async_computation.5 | async-start | bytes 1081344 | tf_op jit(solution)/shard_map/all_gather | solution.py:79
  7.3 118.8 %all-gather.9.cloned.1.call-start = ((), (), s32[]{:S(2)}) async-start(), calls=%async_computation.6 | async-start | bytes 1081344 | tf_op jit(solution)/shard_map/all_gather | solution.py:80
  8.0 185.8 %all-gather.5.cloned.1.call-start = ((), (), s32[]{:S(2)}) async-start(), calls=%async_computation.4 | async-start | bytes 4325376 | tf_op jit(solution)/shard_map/all_gather | solution.py:78
  70.1 57.9 %all-to-all-start.1 = ((bf16[384,8,128]{0,2,1:T(8,128)(2,1)}), bf16[384,8,128]{0,2,1:T(8,128)(2,1)S(1)}, u32[]{:S(2)}, u32[]{:S(2)}) async-start(bf16[384,8,128]{0,2,1:T(8,128)(2,1)} %bitcast.14), calls=%async_computation.1 | async-start | bytes 1572864 | tf_op jit(solution)/shard_map/all_to_all | solution.py:106
  129.0 27.6 %all-to-all-start.2 = ((bf16[384,8,128]{0,2,1:T(8,128)(2,1)}), bf16[384,8,128]{0,2,1:T(8,128)(2,1)S(1)}, u32[]{:S(2)}, u32[]{:S(2)}) async-start(bf16[384,8,128]{0,2,1:T(8,128)(2,1)} %bitcast.90), calls=%async_computation.2 | async-start | bytes 1572864 | tf_op jit(solution)/shard_map/all_to_all | solution.py:107
  133.3 169.3 %all-gather.11.cloned.1.call-start = ((), (), s32[]{:S(2)}) async-start(), calls=%async_computation.7 | async-start | bytes 4325376 | tf_op jit(solution)/shard_map/all_gather | solution.py:124
  200.3 4.6 %copy-start.4 = (f32[64]{0:T(128)S(1)}, f32[64]{0:T(128)}, u32[]{:S(2)}) copy-start(f32[64]{0:T(128)} %param.16) | copy-start | bytes 772
  206.7 29.6 %all-to-all-start = ((bf16[384,8,128]{2,0,1:T(8,128)(2,1)}), bf16[384,8,128]{2,0,1:T(8,128)(2,1)}, u32[]{:S(2)}, u32[]{:S(2)}) async-start(bf16[384,8,128]{2,0,1:T(8,128)(2,1)} %copy.27), calls=%async_computation | async-start | bytes 1572864 | tf_op jit(solution)/shard_map/all_to_all | solution.py:103
  241.2 1.2 copy-start.2
  246.1 1.2 copy-start.2
  250.9 1.2 copy-start.2
  255.7 1.2 copy-start.2
  260.4 1.2 copy-start.2
  265.3 1.2 copy-start.2
  270.6 1.2 copy-start.1
  275.4 1.2 copy-start.1
  280.2 1.2 copy-start.1
  285.0 1.2 copy-start.1
  289.8 1.2 copy-start.1
  294.5 1.2 copy-start.1
  298.9 24.1 %all-to-all-start.3 = ((bf16[8,384,128]{1,2,0:T(8,128)(2,1)}), bf16[8,384,128]{1,2,0:T(8,128)(2,1)S(1)}, u32[]{:S(2)}, u32[]{:S(2)}) async-start(bf16[8,384,128]{1,2,0:T(8,128)(2,1)} %copy.33), calls=%async_computation.3 | async-start | bytes 1572864 | tf_op jit(solution)/shard_map/all_to_all | solution.py:121
Sparse Core Ops, SparseCore 0:
  10.2 56.3 all-gather.6
  69.5 56.4 all-gather.8
  128.9 64.7 all-gather.4
  196.5 66.2 all-gather.10
where the time goes:
time: 336 us; the launch traced here: 335 us
  waiting for transfers between devices  210 us (62%)
  matrix products  55.7 us (17%)
  local copies, waits for them, and re-layouts  23 us (7%)
  starting transfers between devices  16.8 us (5%)
  other arithmetic  15.1 us (4%)
  between operations  13.3 us (4%)
    all_gather x1, waiting for transfers between devices, per_device(): lax.all_gather(k_weight, ('sp', 'dp'), axis=0, tiled=True)  57.6 us
    all_gather x1, waiting for transfers between devices, per_device(): lax.all_gather(v_weight, ('sp', 'dp'), axis=0, tiled=True)  51.6 us
    all_gather x1, waiting for transfers between devices, per_device(): lax.all_gather(q_weight, ('sp', 'dp'), axis=0, tiled=True)  35.9 us
    dot_general x12, matrix products, attend_block(): lax.dot_general(segment, key_rows, (((1,), (1,)), ((), ())), preferred_el...  23.7 us
    all_to_all x1, waiting for transfers between devices, per_device(): lax.all_to_all(values_wide, 'sp', split_axis=1, concat_axis=0, tiled=True)  21.5 us
    all_to_all x1, waiting for transfers between devices, per_device(): lax.all_to_all(queries.reshape(tok_count, q_width), 'sp', split_axis=1, c...  20.6 us
    all_to_all x1, waiting for transfers between devices, per_device(): lax.all_to_all(head_results, 'sp', split_axis=0, concat_axis=1, tiled=True)  20.4 us
    dot_general x12, matrix products, attend_block(): jnp.dot(shares, value_rows, preferred_element_type=jnp.float32)  19.5 us
  transfers between devices with their start and end apart: 8, of which 6 were waited for; matrix products, arithmetic and copies ran while one was open for 26% of the time, Pallas kernels for 0%

commit v1 on v0

--- a/solution.py
+++ b/solution.py
@@ -100,8 +100,16 @@
         (tok_count, kv_heads, group_size, head_width),
     ).reshape(tok_count, q_width)
     q_local, k_local, v_local = (
-        lax.all_to_all(
-            queries.reshape(tok_count, q_width), "sp", split_axis=1, concat_axis=0, tiled=True
+        jnp.concatenate(
+            lax.all_to_all(
+                jnp.stack(
+                    jnp.split(queries.reshape(tok_count, q_width), lax.axis_size("sp"), axis=1)
+                ),
+                "sp",
+                0,
+                0,
+            ),
+            axis=0,
         ),
         lax.all_to_all(keys_wide, "sp", split_axis=1, concat_axis=0, tiled=True),
         lax.all_to_all(values_wide, "sp", split_axis=1, concat_axis=0, tiled=True),

time: 336 us -> 342 us (1.018)
  local copies, waits for them, and re-layouts: 23 us -> 28.1 us
    unnamed x6 -> x21, local copies, waits for them, and re-layouts: 0.01 us -> 5.56 us
  transfers between devices with their start and end apart: 8 -> 8, of which waited for: 6 -> 6; matrix products, arithmetic and copies ran while one was open for 26% -> 27% of each run, Pallas kernels for 0% -> 0%
where the time goes in v1:
time: 342 us; the launch traced here: 341 us
  waiting for transfers between devices  211 us (62%)
  matrix products  55.7 us (16%)
  local copies, waits for them, and re-layouts  28.1 us (8%)
  starting transfers between devices  16.7 us (5%)
  other arithmetic  15.1 us (4%)
  between operations  13.4 us (4%)
    all_gather x1, waiting for transfers between devices, per_device(): lax.all_gather(k_weight, ('sp', 'dp'), axis=0, tiled=True)  57.6 us
    all_gather x1, waiting for transfers between devices, per_device(): lax.all_gather(v_weight, ('sp', 'dp'), axis=0, tiled=True)  51.6 us
    all_gather x1, waiting for transfers between devices, per_device(): lax.all_gather(q_weight, ('sp', 'dp'), axis=0, tiled=True)  35.9 us
    dot_general x12, matrix products, attend_block(): lax.dot_general(segment, key_rows, (((1,), (1,)), ((), ())), preferred_el...  23.7 us
    all_to_all x1, waiting for transfers between devices, per_device(): lax.all_to_all(jnp.stack(jnp.split(queries.reshape(tok_count, q_width), l...  21.7 us
    all_to_all x1, waiting for transfers between devices, per_device(): lax.all_to_all(values_wide, 'sp', split_axis=1, concat_axis=0, tiled=True)  21.6 us
    all_to_all x1, waiting for transfers between devices, per_device(): lax.all_to_all(head_results, 'sp', split_axis=0, concat_axis=1, tiled=True)  20.4 us
    dot_general x12, matrix products, attend_block(): jnp.dot(shares, value_rows, preferred_element_type=jnp.float32)  19.5 us
  transfers between devices with their start and end apart: 8, of which 6 were waited for; matrix products, arithmetic and copies ran while one was open for 27% of the time, Pallas kernels for 0%

profile of v1, /device:TPU:0, one launch (start us, length us, event | category | flops | bytes accessed | tf_op | source)
XLA Modules:
  0.0 340.9 jit_solution(4367314462959582382)
XLA Ops:
  6.5 0.7 all-gather.7.cloned.1.call-update
  7.3 0.7 all-gather.9.cloned.1.call-update
  9.0 57.6 %all-gather.7.cloned.1.call-done = bf16[2048,256]{1,0:T(8,128)(2,1)} async-done(((bf16[64,256]{1,0:T(8,128)(2,1)}), bf16[2048,256]{1,0:T(8,128)(2,1)}) %all-gather.7.cloned.1.call-update) | async-done | bytes 1048592 | tf_op jit(solution)/shard_map/all_gather | solution.py:79
  66.6 1.5 copy.49
  68.1 0.7 multiply_reduce_fusion.3
  69.1 1.0 broadcast_in_dim.14
  70.1 4.3 %all-to-all-start.1 = ((bf16[384,8,128]{0,2,1:T(8,128)(2,1)}), bf16[384,8,128]{0,2,1:T(8,128)(2,1)S(1)}, u32[]{:S(2)}, u32[]{:S(2)}) async-start(bf16[384,8,128]{0,2,1:T(8,128)(2,1)} %bitcast.21), calls=%async_computation.1 | async-start | bytes 1572864 | tf_op jit(solution)/shard_map/all_to_all | solution.py:114
  74.4 51.6 %all-gather.9.cloned.1.call-done = bf16[2048,256]{1,0:T(8,128)(2,1)} async-done(((bf16[64,256]{1,0:T(8,128)(2,1)}), bf16[2048,256]{1,0:T(8,128)(2,1)}) %all-gather.9.cloned.1.call-update) | async-done | bytes 1048592 | tf_op jit(solution)/shard_map/all_gather | solution.py:80
  126.0 2.0 fusion.27
  128.0 1.0 broadcast_in_dim.16
  129.0 4.3 %all-to-all-start.2 = ((bf16[384,8,128]{0,2,1:T(8,128)(2,1)}), bf16[384,8,128]{0,2,1:T(8,128)(2,1)S(1)}, u32[]{:S(2)}, u32[]{:S(2)}) async-start(bf16[384,8,128]{0,2,1:T(8,128)(2,1)} %bitcast.104), calls=%async_computation.2 | async-start | bytes 1572864 | tf_op jit(solution)/shard_map/all_to_all | solution.py:115
  133.9 1.2 copy.50
  135.1 21.6 %all-to-all-done.2 = bf16[384,8,128]{0,2,1:T(8,128)(2,1)S(1)} async-done(((bf16[384,8,128]{0,2,1:T(8,128)(2,1)}), bf16[384,8,128]{0,2,1:T(8,128)(2,1)S(1)}, u32[]{:S(2)}, u32[]{:S(2)}) %all-to-all-start.2) | async-done | bytes 786464 | tf_op jit(solution)/shard_map/all_to_all | solution.py:115
  156.6 1.2 copy.51
  157.8 35.9 %all-gather.5.cloned.1.call-done = bf16[2048,1024]{1,0:T(8,128)(2,1)} async-done(((bf16[64,1024]{1,0:T(8,128)(2,1)}), bf16[2048,1024]{1,0:T(8,128)(2,1)}) %all-gather.5.cloned.1.call-update) | async-done | bytes 4194320 | tf_op jit(solution)/shard_map/all_gather | solution.py:78
  193.8 6.5 %copy.40 = bf16[1024,2048]{1,0:T(8,128)(2,1)} copy(bf16[1024,2048]{0,1:T(8,128)(2,1)} %bitcast.99) | data formatting | bytes 8388608 | tf_op jit(solution)/shard_map/dot_general | solution.py:84
  200.3 4.6 %multiply_reduce_fusion.2 = (f32[384,16]{0,1:T(8,128)S(1)}, f32[384,16,64]{0,2,1:T(8,128)S(1)}) fusion(bf16[16,64,2048]{2,1,0:T(8,128)(2,1)} %bitcast.100, bf16[1,384,2048]{2,1,0:T(8,128)(2,1)S(1)} %copy-done), kind=kOutput, calls=%fused_computation.35 | convolution fusion | flops 1611393024 | bytes 7364608 | tf_op jit(solution)/shard_map/dot_general | solution.py:84
  211.9 4.4 %all-to-all-start = ((bf16[8,384,128]{2,1,0:T(8,128)(2,1)}), bf16[8,384,128]{2,1,0:T(8,128)(2,1)}, u32[]{:S(2)}, u32[]{:S(2)}) async-start(bf16[8,384,128]{2,1,0:T(8,128)(2,1)} %bitcast_dynamic-update-slice_fusion), calls=%async_computation | async-start | bytes 1572864 | tf_op jit(solution)/shard_map/all_to_all | solution.py:104
  216.3 1.7 fusion.36
  218.0 2.8 fusion.35
  220.9 21.7 %all-to-all-done = bf16[8,384,128]{2,1,0:T(8,128)(2,1)} async-done(((bf16[8,384,128]{2,1,0:T(8,128)(2,1)}), bf16[8,384,128]{2,1,0:T(8,128)(2,1)}, u32[]{:S(2)}, u32[]{:S(2)}) %all-to-all-start) | async-done | bytes 786464 | tf_op jit(solution)/shard_map/all_to_all | solution.py:104
  242.6 2.9 fusion.37
  245.5 28.8 %while.20 = (s32[]{:T(128)}, bf16[6,512,64]{1,2,0:T(8,128)(2,1)S(1)}, bf16[6,512,64]{2,1,0:T(8,128)(2,1)}, bf16[3072,64]{1,0:T(8,128)(2,1)S(1)}, bf16[3072,64]{1,0:T(8,128)(2,1)}, /*index=5*/s32[]{:T(128)}) while((s32[]{:T(128)}, bf16[6,512,64]{1,2,0:T(8,128)(2,1)S(1)}, bf16[6,512,64]{2,1,0:T(8,128)(2,1)}, bf16[3072,64]{1,0:T(8,128)(2,1)S(1)}, ...), condition=%wide.region_5.6_spmd, body=%wide.region_2.5_spmd.sunk | while | flops 416840704 | bytes 21834340 | solution.py:63
  245.5 2.0 multiply_reduce_fusion.6
  247.5 1.2 fusion.58
  248.7 1.6 fusion.59
  250.3 2.0 multiply_reduce_fusion.6
  252.3 1.2 fusion.58
  253.5 1.6 fusion.59
  255.1 2.0 multiply_reduce_fusion.6
  257.1 1.2 fusion.58
  258.3 1.6 fusion.59
  259.9 2.0 multiply_reduce_fusion.6
  261.9 1.2 fusion.58
  263.1 1.6 fusion.59
  264.7 2.0 multiply_reduce_fusion.6
  266.7 1.2 fusion.58
  267.9 1.6 fusion.59
  269.5 2.0 multiply_reduce_fusion.6
  271.5 1.2 fusion.58
  272.7 1.6 fusion.59
  274.8 28.7 %while.21 = (s32[]{:T(128)}, bf16[6,512,64]{1,2,0:T(8,128)(2,1)S(1)}, bf16[6,512,64]{2,1,0:T(8,128)(2,1)}, bf16[3072,64]{1,0:T(8,128)(2,1)S(1)}, bf16[3072,64]{1,0:T(8,128)(2,1)}, /*index=5*/s32[]{:T(128)}) while((s32[]{:T(128)}, bf16[6,512,64]{1,2,0:T(8,128)(2,1)S(1)}, bf16[6,512,64]{2,1,0:T(8,128)(2,1)}, bf16[3072,64]{1,0:T(8,128)(2,1)S(1)}, ...), condition=%wide.region_9.10_spmd, body=%wide.region_6.9_spmd.sunk | while | flops 416840704 | bytes 21834340 | solution.py:63
  274.8 2.0 multiply_reduce_fusion.7
  276.8 1.2 fusion.62
  278.0 1.6 fusion.63
  279.6 2.0 multiply_reduce_fusion.7
  281.6 1.2 fusion.62
  282.8 1.6 fusion.63
  284.4 2.0 multiply_reduce_fusion.7
  286.4 1.2 fusion.62
  287.6 1.6 fusion.63
  289.2 2.0 multiply_reduce_fusion.7
  291.2 1.2 fusion.62
  292.4 1.6 fusion.63
  294.0 2.0 multiply_reduce_fusion.7
  296.0 1.2 fusion.62
  297.2 1.6 fusion.63
  298.8 2.0 multiply_reduce_fusion.7
  300.8 1.2 fusion.62
  301.9 1.6 fusion.63
  304.2 1.0 copy.54
  305.2 3.6 %all-to-all-start.3 = ((bf16[8,384,128]{1,2,0:T(8,128)(2,1)}), bf16[8,384,128]{1,2,0:T(8,128)(2,1)S(1)}, u32[]{:S(2)}, u32[]{:S(2)}) async-start(bf16[8,384,128]{1,2,0:T(8,128)(2,1)} %copy.54), calls=%async_computation.3 | async-start | bytes 1572864 | tf_op jit(solution)/shard_map/all_to_all | solution.py:129
  308.8 20.4 %all-to-all-done.3 = bf16[8,384,128]{1,2,0:T(8,128)(2,1)S(1)} async-done(((bf16[8,384,128]{1,2,0:T(8,128)(2,1)}), bf16[8,384,128]{1,2,0:T(8,128)(2,1)S(1)}, u32[]{:S(2)}, u32[]{:S(2)}) %all-to-all-start.3) | async-done | bytes 786464 | tf_op jit(solution)/shard_map/all_to_all | solution.py:129
  329.2 5.2 %fusion.20 = bf16[1,384,2048]{2,1,0:T(8,128)(2,1)} fusion(bf16[384,1024]{0,1:T(8,128)(2,1)S(1)} %bitcast.109, bf16[1024,2048]{0,1:T(8,128)(2,1)} %all-gather.11.cloned.1.call-done), kind=kOutput, calls=%fused_computation.27 | convolution fusion | flops 1611399168 | bytes 6553600 | tf_op jit(solution)/shard_map/dot_general | solution.py:130
  (73 shorter events, 9.9 us)
Async XLA Ops:
  6.5 61.6 %copy-start = (bf16[1,384,2048]{2,1,0:T(8,128)(2,1)S(1)}, bf16[1,384,2048]{2,1,0:T(8,128)(2,1)}, u32[]{:S(2)}) copy-start(bf16[1,384,2048]{2,1,0:T(8,128)(2,1)} %param.11) | copy-start | bytes 4718596
  6.5 62.4 %copy-start.3 = (f32[64]{0:T(128)S(1)}, f32[64]{0:T(128)}, u32[]{:S(2)}) copy-start(f32[64]{0:T(128)} %param.17) | copy-start | bytes 772
  6.5 60.1 %all-gather.7.cloned.1.call-start = ((), (), s32[]{:S(2)}) async-start(), calls=%async_computation.5 | async-start | bytes 1081344 | tf_op jit(solution)/shard_map/all_gather | solution.py:79
  7.3 118.8 %all-gather.9.cloned.1.call-start = ((), (), s32[]{:S(2)}) async-start(), calls=%async_computation.6 | async-start | bytes 1081344 | tf_op jit(solution)/shard_map/all_gather | solution.py:80
  8.0 185.8 %all-gather.5.cloned.1.call-start = ((), (), s32[]{:S(2)}) async-start(), calls=%async_computation.4 | async-start | bytes 4325376 | tf_op jit(solution)/shard_map/all_gather | solution.py:78
  70.1 57.9 %all-to-all-start.1 = ((bf16[384,8,128]{0,2,1:T(8,128)(2,1)}), bf16[384,8,128]{0,2,1:T(8,128)(2,1)S(1)}, u32[]{:S(2)}, u32[]{:S(2)}) async-start(bf16[384,8,128]{0,2,1:T(8,128)(2,1)} %bitcast.21), calls=%async_computation.1 | async-start | bytes 1572864 | tf_op jit(solution)/shard_map/all_to_all | solution.py:114
  129.0 27.6 %all-to-all-start.2 = ((bf16[384,8,128]{0,2,1:T(8,128)(2,1)}), bf16[384,8,128]{0,2,1:T(8,128)(2,1)S(1)}, u32[]{:S(2)}, u32[]{:S(2)}) async-start(bf16[384,8,128]{0,2,1:T(8,128)(2,1)} %bitcast.104), calls=%async_computation.2 | async-start | bytes 1572864 | tf_op jit(solution)/shard_map/all_to_all | solution.py:115
  133.3 175.4 %all-gather.11.cloned.1.call-start = ((), (), s32[]{:S(2)}) async-start(), calls=%async_computation.7 | async-start | bytes 4325376 | tf_op jit(solution)/shard_map/all_gather | solution.py:132
  200.2 4.6 %copy-start.4 = (f32[64]{0:T(128)S(1)}, f32[64]{0:T(128)}, u32[]{:S(2)}) copy-start(f32[64]{0:T(128)} %param.16) | copy-start | bytes 772
  211.9 30.7 %all-to-all-start = ((bf16[8,384,128]{2,1,0:T(8,128)(2,1)}), bf16[8,384,128]{2,1,0:T(8,128)(2,1)}, u32[]{:S(2)}, u32[]{:S(2)}) async-start(bf16[8,384,128]{2,1,0:T(8,128)(2,1)} %bitcast_dynamic-update-slice_fusion), calls=%async_computation | async-start | bytes 1572864 | tf_op jit(solution)/shard_map/all_to_all | solution.py:104
  247.5 1.2 copy-start.2
  252.3 1.2 copy-start.2
  257.1 1.2 copy-start.2
  261.9 1.2 copy-start.2
  266.7 1.2 copy-start.2
  271.5 1.2 copy-start.2
  276.8 1.2 copy-start.1
  281.6 1.2 copy-start.1
  286.4 1.2 copy-start.1
  291.2 1.2 copy-start.1
  296.0 1.2 copy-start.1
  300.8 1.2 copy-start.1
  305.2 24.0 %all-to-all-start.3 = ((bf16[8,384,128]{1,2,0:T(8,128)(2,1)}), bf16[8,384,128]{1,2,0:T(8,128)(2,1)S(1)}, u32[]{:S(2)}, u32[]{:S(2)}) async-start(bf16[8,384,128]{1,2,0:T(8,128)(2,1)} %copy.54), calls=%async_computation.3 | async-start | bytes 1572864 | tf_op jit(solution)/shard_map/all_to_all | solution.py:129
Sparse Core Ops, SparseCore 0:
  10.2 56.3 all-gather.6
  69.5 56.4 all-gather.8
  128.9 64.7 all-gather.4
  196.5 65.7 all-gather.10
